TPU v7x, 32 devices: a whole 2x2x4 slice. The times are simulated.
32 devices in a mesh: dp: 4 (over y, x), kv: 4 (over z), tp: 2 (over core).
Axes of the slice: x: 2, y: 2, z: 4, core: 2. Of those that a mesh axis runs over, the one named last changes fastest.
Arguments:
- stream: bfloat16 [32, 2048], P('dp', ('kv', 'tp')), parts along dimension 0, may hold values from -40 to 40
- old_state: float32 [32, 8, 64, 128], P(('dp', 'kv'), 'tp'), parts along dimension 0, may hold values from -6 to 6
- decay_amounts: float32 [32, 512], P(('dp', 'kv'), 'tp'), parts along dimension 0, may hold values from 0.003 to 1
- first_gain: float32 [2048], replicated, may hold values from 0.1 to 1.9
- first_gate: bfloat16 [2048, 5632], P(None, ('kv', 'tp')), may hold values from -0.125 to 0.125
- first_up: bfloat16 [2048, 5632], P(None, ('kv', 'tp')), may hold values from -0.125 to 0.125
- first_down: bfloat16 [5632, 2048], P(('kv', 'tp')), may hold values from -0.078125 to 0.078125
- mixer_gain: float32 [2048], P('kv'), may hold values from 0.1 to 1.9
- query_weight: bfloat16 [2048, 512], P('kv', 'tp'), may hold values from -0.125 to 0.125
- key_weight: bfloat16 [2048, 512], P('kv', 'tp'), may hold values from -0.125 to 0.125
- decay_weight: bfloat16 [2048, 512], P('kv', 'tp'), may hold values from -0.5 to 0.5
- value_weight: bfloat16 [2048, 1024], P('kv', 'tp'), may hold values from -0.125 to 0.125
- output_gate_weight: bfloat16 [2048, 1024], P('kv', 'tp'), may hold values from -0.125 to 0.125
- head_gain: float32 [1024], P('tp'), may hold values from 0.1 to 1.9
- output_weight: bfloat16 [1024, 2048], P('tp', 'kv'), may hold values from -0.1875 to 0.1875
- second_gain: float32 [2048], replicated, may hold values from 0.1 to 1.9
- second_gate: bfloat16 [2048, 5632], P(None, ('kv', 'tp')), may hold values from -0.125 to 0.125
- second_up: bfloat16 [2048, 5632], P(None, ('kv', 'tp')), may hold values from -0.125 to 0.125
- second_down: bfloat16 [5632, 2048], P(('kv', 'tp')), may hold values from -0.078125 to 0.078125
Outputs:
- mixed_stream: bfloat16 [32, 2048], P('dp', ('kv', 'tp')), parts along dimension 0
- new_state: float32 [32, 8, 64, 128], P(('dp', 'kv'), 'tp'), parts along dimension 0
There are 4 independent parts, one for each index of `dp`. A program takes and returns all parts, laid end to end along the dimension named above; an argument that names none is the same for every part. Nothing has to cross between parts.
All inputs are finite; a program needn't handle non-finite values.
Results may differ from a plain program's by a relative error of at most 0.007.
Values may be sent and summed in bfloat16 or wider, within the bound.
A program may use at most 64 MiB of HBM per device.

v0:
```python
import jax
import jax.numpy as jnp
from jax import lax
from jax.sharding import PartitionSpec as P

D = 2048
EPSILON = 1e-06
GATE_SOFTNESS = 16.0


def half_block(stream, norm_gain, w_gate, w_up, w_down):
    wide = lax.all_gather(stream, ("kv", "tp"), axis=1, tiled=True).astype(jnp.float32)
    scaled = (wide * norm_gain).astype(jnp.bfloat16)
    gate_acc = jnp.dot(scaled, w_gate, preferred_element_type=jnp.float32)
    up_acc = jnp.dot(scaled, w_up, preferred_element_type=jnp.float32)
    square_acc = jnp.sum(wide * wide, axis=1)
    row_scale = lax.rsqrt(square_acc / norm_gain.shape[0] + EPSILON)[:, None]
    hidden = (jax.nn.silu(gate_acc * row_scale) * (up_acc * row_scale)).astype(jnp.bfloat16)
    partial_out = jnp.dot(hidden, w_down, preferred_element_type=jnp.float32)
    summed = lax.psum_scatter(partial_out, ("kv", "tp"), scatter_dimension=1, tiled=True)
    return (stream.astype(jnp.float32) + 0.5 * summed).astype(jnp.bfloat16)


def body(
    stream,
    old_state,
    decay_amounts,
    first_gain,
    first_gate,
    first_up,
    first_down,
    mixer_gain,
    query_weight,
    key_weight,
    decay_weight,
    value_weight,
    output_gate_weight,
    head_gain,
    output_weight,
    second_gain,
    second_gate,
    second_up,
    second_down,
):
    middle = half_block(stream, first_gain, first_gate, first_up, first_down)
    paired_cols = lax.all_gather(middle, "tp", axis=1, tiled=True)
    wide_cols = paired_cols.astype(jnp.float32)
    scaled = (wide_cols * mixer_gain).astype(jnp.bfloat16)
    query_part = jnp.dot(scaled, query_weight, preferred_element_type=jnp.float32)
    key_part = jnp.dot(scaled, key_weight, preferred_element_type=jnp.float32)
    decay_part = jnp.dot(scaled, decay_weight, preferred_element_type=jnp.float32)
    value_part = jnp.dot(scaled, value_weight, preferred_element_type=jnp.float32)
    outgate_part = jnp.dot(scaled, output_gate_weight, preferred_element_type=jnp.float32)
    local_rows = old_state.shape[0]
    local_heads = old_state.shape[1]
    key_dim = old_state.shape[2]
    value_dim = old_state.shape[3]
    query_sum, key_sum, decay_sum, value_sum, outgate_sum, own_squares = (
        lax.psum_scatter(query_part, "kv", scatter_dimension=0, tiled=True),
        lax.psum_scatter(key_part, "kv", scatter_dimension=0, tiled=True),
        lax.psum_scatter(decay_part, "kv", scatter_dimension=0, tiled=True),
        lax.psum_scatter(value_part, "kv", scatter_dimension=0, tiled=True),
        lax.psum_scatter(outgate_part, "kv", scatter_dimension=0, tiled=True),
        lax.psum_scatter(
            jnp.sum(wide_cols * wide_cols, axis=1), "kv", scatter_dimension=0, tiled=True
        ),
    )
    row_scale = lax.rsqrt(own_squares / D + EPSILON)[:, None]
    query = (query_sum * row_scale * key_dim ** (-0.5)).reshape(local_rows, local_heads, key_dim)
    keys = (key_sum * row_scale).reshape(local_rows, local_heads, key_dim)
    gate_logits = (decay_sum * row_scale).reshape(local_rows, local_heads, key_dim)
    values = (value_sum * row_scale).reshape(local_rows, local_heads, value_dim)
    decay_logarithm = jax.nn.log_sigmoid(gate_logits) / GATE_SOFTNESS - decay_amounts.reshape(
        local_rows, local_heads, key_dim
    )
    new_state = (
        jnp.exp(decay_logarithm)[..., None] * old_state + keys[..., None] * values[:, :, None, :]
    )
    readout = jnp.einsum("bhk,bhkv->bhv", query, new_state, precision=lax.Precision.HIGHEST)
    normed = readout * lax.rsqrt(jnp.mean(readout * readout, axis=-1, keepdims=True) + EPSILON)
    mixed_heads = (
        normed.reshape(local_rows, local_heads * value_dim)
        * head_gain
        * jax.nn.silu(outgate_sum * row_scale)
    ).astype(jnp.bfloat16)
    projected = jnp.dot(
        lax.all_gather(mixed_heads, "kv", axis=0, tiled=True),
        output_weight,
        preferred_element_type=jnp.float32,
    ).astype(jnp.bfloat16)
    attention_out = lax.psum_scatter(
        lax.optimization_barrier(projected).astype(jnp.float32).astype(jnp.bfloat16),
        "tp",
        scatter_dimension=1,
        tiled=True,
    ).astype(jnp.float32)
    after = (middle.astype(jnp.float32) + attention_out).astype(jnp.bfloat16)
    mixed_stream = half_block(after, second_gain, second_gate, second_up, second_down)
    return (mixed_stream, new_state)


def solution(mesh):
    in_specs = (
        P("dp", ("kv", "tp")),
        P(("dp", "kv"), "tp", None, None),
        P(("dp", "kv"), "tp"),
        P(),
        P(None, ("kv", "tp")),
        P(None, ("kv", "tp")),
        P(("kv", "tp"), None),
        P("kv"),
        P("kv", "tp"),
        P("kv", "tp"),
        P("kv", "tp"),
        P("kv", "tp"),
        P("kv", "tp"),
        P("tp"),
        P("tp", "kv"),
        P(),
        P(None, ("kv", "tp")),
        P(None, ("kv", "tp")),
        P(("kv", "tp"), None),
    )
    out_specs = (P("dp", ("kv", "tp")), P(("dp", "kv"), "tp", None, None))
    return jax.shard_map(body, mesh=mesh, in_specs=in_specs, out_specs=out_specs, check_vma=False)
```

profile of v0, /device:TPU:0, one launch (start us, length us, event | category | flops | bytes accessed | tf_op | source)
XLA Modules:
  0.0 171.4 jit_solution(4641886258188548074)
XLA Ops:
  7.2 16.1 %all_gather.12 = bf16[8,2048]{1,0:T(8,128)(2,1)S(1)} all-gather(bf16[8,256]{1,0:T(8,128)(2,1)} %param.19), channel_id=1, replica_groups=mesh['dp'=4,'kv'=4,'tp'=2] {'kv','tp'}, dimensions={1}, use_global_device_ids=true | all-gather | bytes 36864 | tf_op jit(solution)/shard_map/all_gather | solution.py:12
  23.3 0.1 fusion.7
  23.4 2.7 %convolution_multiply_fusion.3 = f32[8,704]{1,0:T(8,128)S(1)} fusion(bf16[2048,704]{0,1:T(8,128)(2,1)} %param.23, bf16[8,2048]{1,0:T(8,128)(2,1)S(1)} %all_gather.12, f32[2048]{0:T(1024)} %param.22, f32[8]{0:T(128)S(1)} %add_rsqrt_fusion.2), kind=kOutput, calls=%fused_computation.5 | convolution fusion | flops 23123456 | bytes 2947104 | tf_op jit(solution)/shard_map/dot_general | solution.py:14
  26.2 4.2 %fusion.5 = f32[8,2048]{1,0:T(8,128)} fusion(bf16[704,2048]{1,0:T(8,128)(2,1)S(1)} %copy-done, bf16[2048,704]{0,1:T(8,128)(2,1)} %param.24, bf16[8,2048]{1,0:T(8,128)(2,1)S(1)} %all_gather.12, f32[2048]{0:T(1024)S(1)} %copy-done.4, f32[8,704]{1,0:T(8,128)S(1)} %convolution_multiply_fusion.3, f32[8]{0:T(128)S(1)} %add_rsqrt_fusion.2), kind=kOutput, calls=%fused_computation.9 | convolution fusion | flops 46225920 | bytes 5896224 | tf_op jit(solution)/shard_map/dot_general | solution.py:19
  30.5 0.1 reshape.62
  30.5 0.6 dynamic-slice
  31.1 30.9 %reduce-scatter.4.cloned.1.call-done = f32[8,256]{1,0:T(8,128)} async-done(((f32[8,2048]{1,0:T(8,128)}), f32[8,256]{1,0:T(8,128)}) %reduce-scatter.4.cloned.1.call-update) | async-done | bytes 8208 | tf_op jit(solution)/shard_map/reduce_scatter | solution.py:20
  62.0 0.7 add_convert_fusion.2
  62.7 1.8 %all_gather.13 = bf16[8,512]{1,0:T(8,128)(2,1)S(1)} all-gather(bf16[8,256]{1,0:T(8,128)(2,1)S(1)} %add_convert_fusion.2), channel_id=1, replica_groups=mesh['dp'=4,'kv'=4,'tp'=2] {'tp'}, dimensions={1}, use_global_device_ids=true | all-gather | bytes 12288 | tf_op jit(solution)/shard_map/all_gather | solution.py:46
  64.5 0.1 fusion.27
  64.7 1.1 fusion.49
  65.8 1.1 fusion.47
  66.9 1.1 fusion.51
  68.0 0.2 fusion.45
  68.1 1.2 fusion.43
  70.0 16.6 %all-reduce.6 = (f32[8]{0:T(128)S(1)}, f32[8,512]{1,0:T(8,128)S(1)}, f32[8,256]{1,0:T(8,128)S(1)}, f32[8,512]{1,0:T(8,128)S(1)}, f32[8,256]{1,0:T(8,128)S(1)}, /*index=5*/f32[8,256]{1,0:T(8,128)S(1)}) all-reduce(f32[8]{0:T(128)S(1)} %fusion.27, f32[8,512]{1,0:T(8,128)S(1)} %fusion.43, ...), channel_id=4, replica_groups=mesh['dp'=4,'kv'=4,'tp'=2] {'kv'}, use_global_device_ids=true, to_apply=%region_4.5.clone | all-reduce | flops 14344 | bytes 114752
  86.9 0.1 neg.41
  87.0 0.1 mul.191
  87.2 1.1 multiply_add_fusion
  88.4 0.3 fusion.55
  88.7 0.1 multiply_reduce_fusion
  88.8 0.1 fusion.40
  89.0 11.9 %all-gather = bf16[4,2,512]{2,1,0:T(2,128)(2,1)S(1)} all-gather(bf16[1,2,512]{2,1,0:T(2,128)(2,1)S(1)} %fusion.40), channel_id=1, replica_groups=mesh['dp'=4,'kv'=4,'tp'=2] {'kv'}, dimensions={0}, use_global_device_ids=true | all-gather | bytes 10240 | tf_op jit(solution)/shard_map/all_gather | solution.py:87
  100.9 1.8 %convolution_convert_fusion = bf16[8,512]{1,0:T(8,128)(2,1)} fusion(bf16[8,512]{1,0:T(8,128)(2,1)S(1)} %reshape.65, bf16[512,512]{1,0:T(8,128)(2,1)} %param.33), kind=kOutput, calls=%fused_computation.10 | convolution fusion | flops 4198400 | bytes 540672 | tf_op jit(solution)/shard_map/dot_general | solution.py:86
  102.8 6.4 %reduce-scatter.6.cloned.1.call-done = bf16[8,256]{1,0:T(8,128)(2,1)} async-done(((bf16[8,512]{1,0:T(8,128)(2,1)}), bf16[8,256]{1,0:T(8,128)(2,1)}) %reduce-scatter.6.cloned.1.call-update) | async-done | bytes 4112 | tf_op jit(solution)/shard_map/reduce_scatter | solution.py:91
  109.2 0.7 add_convert_fusion.1
  109.8 14.3 %all_gather.15 = bf16[8,2048]{1,0:T(8,128)(2,1)S(1)} all-gather(bf16[8,256]{1,0:T(8,128)(2,1)S(1)} %add_convert_fusion.1), channel_id=1, replica_groups=mesh['dp'=4,'kv'=4,'tp'=2] {'kv','tp'}, dimensions={1}, use_global_device_ids=true | all-gather | bytes 36864 | tf_op jit(solution)/shard_map/all_gather | solution.py:12
  124.2 0.1 fusion.9
  124.3 2.7 %convolution_multiply_fusion.1 = f32[8,704]{1,0:T(8,128)S(1)} fusion(bf16[2048,704]{0,1:T(8,128)(2,1)} %param.35, bf16[8,2048]{1,0:T(8,128)(2,1)S(1)} %all_gather.15, f32[2048]{0:T(1024)S(1)} %copy-done.5, f32[8]{0:T(128)S(1)} %add_rsqrt_fusion.1), kind=kOutput, calls=%fused_computation.2 | convolution fusion | flops 23123456 | bytes 2947104 | tf_op jit(solution)/shard_map/dot_general | solution.py:14
  127.0 5.0 %fusion.4 = f32[8,2048]{1,0:T(8,128)} fusion(bf16[704,2048]{1,0:T(8,128)(2,1)} %param.37, bf16[2048,704]{0,1:T(8,128)(2,1)} %param.36, bf16[8,2048]{1,0:T(8,128)(2,1)S(1)} %all_gather.15, f32[2048]{0:T(1024)S(1)} %copy-done.5, f32[8,704]{1,0:T(8,128)S(1)} %convolution_multiply_fusion.1, f32[8]{0:T(128)S(1)} %add_rsqrt_fusion.1), kind=kOutput, calls=%fused_computation.8 | convolution fusion | flops 46225920 | bytes 5896224 | tf_op jit(solution)/shard_map/dot_general | solution.py:19
  132.0 31.5 %reduce-scatter.8.cloned.1.call-done = f32[8,256]{1,0:T(8,128)} async-done(((f32[8,2048]{1,0:T(8,128)}), f32[8,256]{1,0:T(8,128)}) %reduce-scatter.8.cloned.1.call-update) | async-done | bytes 8208 | tf_op jit(solution)/shard_map/reduce_scatter | solution.py:20
  163.5 1.3 add_convert_fusion
  (37 shorter events, 0.7 us)
Async XLA Ops:
  7.2 19.0 %copy-start = (bf16[704,2048]{1,0:T(8,128)(2,1)S(1)}, bf16[704,2048]{1,0:T(8,128)(2,1)}, u32[]{:S(2)}) copy-start(bf16[704,2048]{1,0:T(8,128)(2,1)} %param.25) | copy-start | bytes 8650756
  7.2 18.9 %copy-start.4 = (f32[2048]{0:T(1024)S(1)}, f32[2048]{0:T(1024)}, u32[]{:S(2)}) copy-start(f32[2048]{0:T(1024)} %param.22) | copy-start | bytes 24580
  7.2 54.8 %reduce-scatter.4.cloned.1.call-start = ((), (), s32[]{:S(2)}) async-start(), calls=%async_computation.3 | async-start | bytes 73728 | tf_op jit(solution)/shard_map/reduce_scatter | solution.py:20
  26.1 4.3 %copy-start.7 = (f32[2,256]{1,0:T(2,128)S(1)}, f32[2,256]{1,0:T(2,128)}, u32[]{:S(2)}) copy-start(f32[2,256]{1,0:T(2,128)} %param.21) | copy-start | bytes 6148
  26.1 4.4 %copy-start.9 = (u32[32]{0:T(128)S(1)}, u32[32]{0:T(128)}, u32[]{:S(2)}) copy-start(u32[32]{0:T(128)} %constant.35) | copy-start | bytes 388
  26.2 35.9 %copy-start.6 = (bf16[8,256]{1,0:T(8,128)(2,1)S(1)}, bf16[8,256]{1,0:T(8,128)(2,1)}, u32[]{:S(2)}) copy-start(bf16[8,256]{1,0:T(8,128)(2,1)} %param.19) | copy-start | bytes 12292
  26.2 38.5 %copy-start.3 = (f32[512]{0:T(512)S(1)}, f32[512]{0:T(512)}, u32[]{:S(2)}) copy-start(f32[512]{0:T(512)} %param.26) | copy-start | bytes 6148
  26.2 41.8 %copy-start.2 = (bf16[512,512]{1,0:T(8,128)(2,1)S(1)}, bf16[512,512]{1,0:T(8,128)(2,1)}, u32[]{:S(2)}) copy-start(bf16[512,512]{1,0:T(8,128)(2,1)} %param.30) | copy-start | bytes 1572868
  30.4 58.5 %copy-start.8 = (f32[512]{0:T(512)S(1)}, f32[512]{0:T(512)}, u32[]{:S(2)}) copy-start(f32[512]{0:T(512)} %param.32) | copy-start | bytes 6148
  30.4 93.9 %copy-start.5 = (f32[2048]{0:T(1024)S(1)}, f32[2048]{0:T(1024)}, u32[]{:S(2)}) copy-start(f32[2048]{0:T(1024)} %param.34) | copy-start | bytes 24580
  30.4 78.8 %reduce-scatter.6.cloned.1.call-start = ((), (), s32[]{:S(2)}) async-start(), calls=%async_computation.4 | async-start | bytes 12288 | tf_op jit(solution)/shard_map/reduce_scatter | solution.py:91
  88.4 43.6 %copy-start.1 = (f32[2,4,64,128]{3,2,1,0:T(8,128)}, f32[2,4,64,128]{3,2,1,0:T(8,128)S(1)}, u32[]{:S(2)}) copy-start(f32[2,4,64,128]{3,2,1,0:T(8,128)S(1)} %multiply_add_fusion) | copy-start | bytes 786436
  102.7 60.8 %reduce-scatter.8.cloned.1.call-start = ((), (), s32[]{:S(2)}) async-start(), calls=%async_computation.5 | async-start | bytes 73728 | tf_op jit(solution)/shard_map/reduce_scatter | solution.py:20
Sparse Core Ops, SparseCore 0:
  30.5 31.4 reduce-scatter.3
  102.9 6.2 reduce-scatter.5
  132.1 31.3 reduce-scatter.7
where the time goes:
time: 172 us; the launch traced here: 171 us
  waiting for transfers between devices  68.8 us (40%)
  blocking collectives  60.8 us (35%)
  matrix products  21.3 us (12%)
  between operations  14.6 us (8%)
  other arithmetic  4.73 us (3%)
    reduce_scatter x2, waiting for transfers between devices, half_block(): lax.psum_scatter(partial_out, ('kv', 'tp'), scatter_dimension=1, tiled=True)  62.4 us
    all_gather x2, blocking collectives, half_block(): lax.all_gather(stream, ('kv', 'tp'), axis=1, tiled=True).astype(jnp.float32)  30.4 us
    unnamed x1, blocking collectives  16.6 us
    all_gather x1, blocking collectives, body(): lax.all_gather(mixed_heads, 'kv', axis=0, tiled=True)  11.9 us
    dot_general x2, matrix products, half_block(): partial_out = jnp.dot(hidden, w_down, preferred_element_type=jnp.float32)  9.16 us
    reduce_scatter x1, waiting for transfers between devices, body(): lax.psum_scatter(lax.optimization_barrier(projected).astype(jnp.float32)....  6.35 us
    dot_general x2, matrix products, half_block(): gate_acc = jnp.dot(scaled, w_gate, preferred_element_type=jnp.float32)  5.33 us
  transfers between devices with their start and end apart: 3, of which 3 were waited for; matrix products, arithmetic and copies ran while one was open for 0% of the time, Pallas kernels for 0%

commit v1 on v0

--- a/solution.py
+++ b/solution.py
@@ -9,7 +9,7 @@
 
 
 def half_block(stream, norm_gain, w_gate, w_up, w_down):
-    wide = lax.all_gather(stream, ("kv", "tp"), axis=1, tiled=True).astype(jnp.float32)
+    wide = jnp.concatenate(lax.all_gather(stream, axis_name=("kv", "tp")), 1).astype(jnp.float32)
     scaled = (wide * norm_gain).astype(jnp.bfloat16)
     gate_acc = jnp.dot(scaled, w_gate, preferred_element_type=jnp.float32)
     up_acc = jnp.dot(scaled, w_up, preferred_element_type=jnp.float32)

time: 172 us -> 172 us (level)
  no operation moved by 1% of the time
where the time goes in v1:
time: 172 us; the launch traced here: 171 us
  waiting for transfers between devices  68.8 us (40%)
  blocking collectives  60.8 us (35%)
  matrix products  21.3 us (12%)
  between operations  14.6 us (8%)
  other arithmetic  4.74 us (3%)
    reduce_scatter x2, waiting for transfers between devices, half_block(): lax.psum_scatter(partial_out, ('kv', 'tp'), scatter_dimension=1, tiled=True)  62.4 us
    all_gather x2, blocking collectives, half_block(): lax.all_gather(stream, axis_name=('kv', 'tp'))  30.4 us
    unnamed x1, blocking collectives  16.6 us
    all_gather x1, blocking collectives, body(): lax.all_gather(mixed_heads, 'kv', axis=0, tiled=True)  11.9 us
    dot_general x2, matrix products, half_block(): partial_out = jnp.dot(hidden, w_down, preferred_element_type=jnp.float32)  9.16 us
    reduce_scatter x1, waiting for transfers between devices, body(): lax.psum_scatter(lax.optimization_barrier(projected).astype(jnp.float32)....  6.35 us
    dot_general x2, matrix products, half_block(): gate_acc = jnp.dot(scaled, w_gate, preferred_element_type=jnp.float32)  5.33 us
  transfers between devices with their start and end apart: 3, of which 3 were waited for; matrix products, arithmetic and copies ran while one was open for 0% of the time, Pallas kernels for 0%

profile of v1, /device:TPU:0, one launch (start us, length us, event | category | flops | bytes accessed | tf_op | source)
XLA Modules:
  0.0 171.4 jit_solution(16769596915024171658)
XLA Ops:
  7.2 16.1 %all-gather = bf16[64,256]{1,0:T(8,128)(2,1)S(1)} all-gather(bf16[8,256]{1,0:T(8,128)(2,1)} %param.19), channel_id=2, replica_groups=mesh['dp'=4,'kv'=4,'tp'=2] {'kv','tp'}, dimensions={0}, use_global_device_ids=true | all-gather | bytes 36864 | tf_op jit(solution)/shard_map/all_gather | solution.py:12
  23.3 0.1 multiply_reduce_fusion.1
  23.4 2.7 %convolution_multiply_fusion.3 = f32[8,704]{1,0:T(8,128)S(1)} fusion(bf16[2048,704]{0,1:T(8,128)(2,1)} %param.23, f32[8]{0:T(128)S(1)} %add_rsqrt_fusion.2, f32[8,2048]{1,0:T(8,128)S(1)} %bitcast.47, f32[2048]{0:T(1024)} %param.22), kind=kOutput, calls=%fused_computation.5 | convolution fusion | flops 23107072 | bytes 2979872 | tf_op jit(solution)/shard_map/dot_general | solution.py:14
  26.2 4.2 %fusion.5 = f32[8,2048]{1,0:T(8,128)} fusion(bf16[704,2048]{1,0:T(8,128)(2,1)S(1)} %copy-done, bf16[2048,704]{0,1:T(8,128)(2,1)} %param.24, f32[8,704]{1,0:T(8,128)S(1)} %convolution_multiply_fusion.3, f32[8]{0:T(128)S(1)} %add_rsqrt_fusion.2, f32[8,2048]{1,0:T(8,128)S(1)} %bitcast.48, f32[2048]{0:T(1024)S(1)} %copy-done.4), kind=kOutput, calls=%fused_computation.9 | convolution fusion | flops 46209536 | bytes 5928992 | tf_op jit(solution)/shard_map/dot_general | solution.py:19
  30.5 0.1 reshape.70
  30.6 0.6 dynamic-slice
  31.1 30.9 %reduce-scatter.4.cloned.1.call-done = f32[8,256]{1,0:T(8,128)} async-done(((f32[8,2048]{1,0:T(8,128)}), f32[8,256]{1,0:T(8,128)}) %reduce-scatter.4.cloned.1.call-update) | async-done | bytes 8208 | tf_op jit(solution)/shard_map/reduce_scatter | solution.py:20
  62.0 0.7 add_convert_fusion.2
  62.7 1.8 %all_gather.20 = bf16[8,512]{1,0:T(8,128)(2,1)S(1)} all-gather(bf16[8,256]{1,0:T(8,128)(2,1)S(1)} %add_convert_fusion.2), channel_id=1, replica_groups=mesh['dp'=4,'kv'=4,'tp'=2] {'tp'}, dimensions={1}, use_global_device_ids=true | all-gather | bytes 12288 | tf_op jit(solution)/shard_map/all_gather | solution.py:46
  64.5 0.1 fusion.17
  64.7 1.1 fusion.39
  65.8 1.1 fusion.37
  66.9 1.1 fusion.41
  68.0 0.2 fusion.35
  68.1 1.2 fusion.33
  70.0 16.6 %all-reduce.6 = (f32[8]{0:T(128)S(1)}, f32[8,512]{1,0:T(8,128)S(1)}, f32[8,256]{1,0:T(8,128)S(1)}, f32[8,512]{1,0:T(8,128)S(1)}, f32[8,256]{1,0:T(8,128)S(1)}, /*index=5*/f32[8,256]{1,0:T(8,128)S(1)}) all-reduce(f32[8]{0:T(128)S(1)} %fusion.17, f32[8,512]{1,0:T(8,128)S(1)} %fusion.33, ...), channel_id=6, replica_groups=mesh['dp'=4,'kv'=4,'tp'=2] {'kv'}, use_global_device_ids=true, to_apply=%region_4.5.clone | all-reduce | flops 14344 | bytes 114752
  86.9 0.1 neg.41
  87.0 0.1 mul.195
  87.2 1.1 multiply_add_fusion
  88.4 0.3 fusion.45
  88.7 0.1 multiply_reduce_fusion.2
  88.9 0.1 fusion.30
  89.0 11.9 %all-gather.2 = bf16[4,2,512]{2,1,0:T(2,128)(2,1)S(1)} all-gather(bf16[1,2,512]{2,1,0:T(2,128)(2,1)S(1)} %fusion.30), channel_id=1, replica_groups=mesh['dp'=4,'kv'=4,'tp'=2] {'kv'}, dimensions={0}, use_global_device_ids=true | all-gather | bytes 10240 | tf_op jit(solution)/shard_map/all_gather | solution.py:87
  100.9 1.8 %convolution_convert_fusion = bf16[8,512]{1,0:T(8,128)(2,1)} fusion(bf16[8,512]{1,0:T(8,128)(2,1)S(1)} %reshape.81, bf16[512,512]{1,0:T(8,128)(2,1)} %param.33), kind=kOutput, calls=%fused_computation.10 | convolution fusion | flops 4198400 | bytes 540672 | tf_op jit(solution)/shard_map/dot_general | solution.py:86
  102.8 6.4 %reduce-scatter.6.cloned.1.call-done = bf16[8,256]{1,0:T(8,128)(2,1)} async-done(((bf16[8,512]{1,0:T(8,128)(2,1)}), bf16[8,256]{1,0:T(8,128)(2,1)}) %reduce-scatter.6.cloned.1.call-update) | async-done | bytes 4112 | tf_op jit(solution)/shard_map/reduce_scatter | solution.py:91
  109.2 0.7 add_convert_fusion.1
  109.8 14.3 %all-gather.1 = bf16[64,256]{1,0:T(8,128)(2,1)S(1)} all-gather(bf16[8,256]{1,0:T(8,128)(2,1)S(1)} %add_convert_fusion.1), channel_id=3, replica_groups=mesh['dp'=4,'kv'=4,'tp'=2] {'kv','tp'}, dimensions={0}, use_global_device_ids=true | all-gather | bytes 36864 | tf_op jit(solution)/shard_map/all_gather | solution.py:12
  124.2 0.1 multiply_reduce_fusion
  124.3 2.7 %convolution_multiply_fusion.1 = f32[8,704]{1,0:T(8,128)S(1)} fusion(bf16[2048,704]{0,1:T(8,128)(2,1)} %param.35, f32[8]{0:T(128)S(1)} %add_rsqrt_fusion.1, f32[8,2048]{1,0:T(8,128)S(1)} %bitcast.49, f32[2048]{0:T(1024)S(1)} %copy-done.5), kind=kOutput, calls=%fused_computation.2 | convolution fusion | flops 23107072 | bytes 2979872 | tf_op jit(solution)/shard_map/dot_general | solution.py:14
  127.0 5.0 %fusion.4 = f32[8,2048]{1,0:T(8,128)} fusion(bf16[704,2048]{1,0:T(8,128)(2,1)} %param.37, bf16[2048,704]{0,1:T(8,128)(2,1)} %param.36, f32[8,704]{1,0:T(8,128)S(1)} %convolution_multiply_fusion.1, f32[8]{0:T(128)S(1)} %add_rsqrt_fusion.1, f32[8,2048]{1,0:T(8,128)S(1)} %bitcast.50, f32[2048]{0:T(1024)S(1)} %copy-done.5), kind=kOutput, calls=%fused_computation.8 | convolution fusion | flops 46209536 | bytes 5928992 | tf_op jit(solution)/shard_map/dot_general | solution.py:19
  132.0 31.5 %reduce-scatter.8.cloned.1.call-done = f32[8,256]{1,0:T(8,128)} async-done(((f32[8,2048]{1,0:T(8,128)}), f32[8,256]{1,0:T(8,128)}) %reduce-scatter.8.cloned.1.call-update) | async-done | bytes 8208 | tf_op jit(solution)/shard_map/reduce_scatter | solution.py:20
  163.6 1.3 add_convert_fusion
  (39 shorter events, 0.7 us)
Async XLA Ops:
  7.2 19.0 %copy-start = (bf16[704,2048]{1,0:T(8,128)(2,1)S(1)}, bf16[704,2048]{1,0:T(8,128)(2,1)}, u32[]{:S(2)}) copy-start(bf16[704,2048]{1,0:T(8,128)(2,1)} %param.25) | copy-start | bytes 8650756
  7.2 18.9 %copy-start.4 = (f32[2048]{0:T(1024)S(1)}, f32[2048]{0:T(1024)}, u32[]{:S(2)}) copy-start(f32[2048]{0:T(1024)} %param.22) | copy-start | bytes 24580
  7.2 54.8 %reduce-scatter.4.cloned.1.call-start = ((), (), s32[]{:S(2)}) async-start(), calls=%async_computation.3 | async-start | bytes 73728 | tf_op jit(solution)/shard_map/reduce_scatter | solution.py:20
  26.1 4.3 %copy-start.7 = (f32[2,256]{1,0:T(2,128)S(1)}, f32[2,256]{1,0:T(2,128)}, u32[]{:S(2)}) copy-start(f32[2,256]{1,0:T(2,128)} %param.21) | copy-start | bytes 6148
  26.2 4.4 %copy-start.9 = (u32[32]{0:T(128)S(1)}, u32[32]{0:T(128)}, u32[]{:S(2)}) copy-start(u32[32]{0:T(128)} %constant.35) | copy-start | bytes 388
  26.2 35.9 %copy-start.6 = (bf16[8,256]{1,0:T(8,128)(2,1)S(1)}, bf16[8,256]{1,0:T(8,128)(2,1)}, u32[]{:S(2)}) copy-start(bf16[8,256]{1,0:T(8,128)(2,1)} %param.19) | copy-start | bytes 12292
  26.2 38.5 %copy-start.3 = (f32[512]{0:T(512)S(1)}, f32[512]{0:T(512)}, u32[]{:S(2)}) copy-start(f32[512]{0:T(512)} %param.26) | copy-start | bytes 6148
  26.2 41.8 %copy-start.2 = (bf16[512,512]{1,0:T(8,128)(2,1)S(1)}, bf16[512,512]{1,0:T(8,128)(2,1)}, u32[]{:S(2)}) copy-start(bf16[512,512]{1,0:T(8,128)(2,1)} %param.30) | copy-start | bytes 1572868
  30.4 58.5 %copy-start.8 = (f32[512]{0:T(512)S(1)}, f32[512]{0:T(512)}, u32[]{:S(2)}) copy-start(f32[512]{0:T(512)} %param.32) | copy-start | bytes 6148
  30.4 94.0 %copy-start.5 = (f32[2048]{0:T(1024)S(1)}, f32[2048]{0:T(1024)}, u32[]{:S(2)}) copy-start(f32[2048]{0:T(1024)} %param.34) | copy-start | bytes 24580
  30.4 78.8 %reduce-scatter.6.cloned.1.call-start = ((), (), s32[]{:S(2)}) async-start(), calls=%async_computation.4 | async-start | bytes 12288 | tf_op jit(solution)/shard_map/reduce_scatter | solution.py:91
  88.4 43.6 %copy-start.1 = (f32[2,4,64,128]{3,2,1,0:T(8,128)}, f32[2,4,64,128]{3,2,1,0:T(8,128)S(1)}, u32[]{:S(2)}) copy-start(f32[2,4,64,128]{3,2,1,0:T(8,128)S(1)} %multiply_add_fusion) | copy-start | bytes 786436
  102.8 60.8 %reduce-scatter.8.cloned.1.call-start = ((), (), s32[]{:S(2)}) async-start(), calls=%async_computation.5 | async-start | bytes 73728 | tf_op jit(solution)/shard_map/reduce_scatter | solution.py:20
Sparse Core Ops, SparseCore 0:
  30.5 31.4 reduce-scatter.3
  102.9 6.2 reduce-scatter.5
  132.1 31.3 reduce-scatter.7
